TPU v7x, 128 devices: a whole 4x4x4 slice. The times are simulated.
128 devices in a mesh: rep: 2 (over z_hi), fs: 32 (over z_lo, y, x), tp: 2 (over core).
Axes of the slice: x: 4, y: 4, z: 4 (z_hi: 2, z_lo: 2; z = z_hi * 2 + z_lo), core: 2. Of those that a mesh axis runs over, the one named last changes fastest.
Arguments:
- resid: bfloat16 [65536, 2048], P(('rep', 'fs'), 'tp'), may hold values from -6 to 6
- gain_mix_in: float32 [2048], replicated, may hold values from 0.1 to 1.9
- u_weight: float32 [2048, 1024], P('fs', 'tp'), may hold values from -0.125 to 0.125
- v_weight: float32 [2048, 1024], P('fs', 'tp'), may hold values from -0.125 to 0.125
- u_scale: float32 [1024], P('tp'), may hold values from 0.5 to 2
- v_scale: float32 [1024], P('tp'), may hold values from 0.3 to 3
- v_gain: float32 [1024], P('tp'), may hold values from 0.1 to 1.9
- mix_matrix: float32 [16, 128, 128], P('tp'), may hold values from -0.5 to 0.5
- mix_bias: float32 [16, 128], P('tp'), may hold values from 0.1 to 1.9
- out_weight: float32 [1024, 2048], P('tp', 'fs'), may hold values from -0.1875 to 0.1875
- out_scale: float32 [2048], P('fs'), may hold values from 0.3 to 3
- gain_mix_out: float32 [2048], replicated, may hold values from 0.1 to 1.9
- gain_ffn_in: float32 [2048], replicated, may hold values from 0.1 to 1.9
- up_weight: float32 [2048, 4096], P('fs', 'tp'), may hold values from -0.125 to 0.125
- up_scale: float32 [4096], P('tp'), may hold values from 0.5 to 2
- down_weight: float32 [4096, 2048], P('tp', 'fs'), may hold values from -0.09375 to 0.09375
- down_scale: float32 [2048], P('fs'), may hold values from 0.3 to 3
- gain_ffn_out: float32 [2048], replicated, may hold values from 0.1 to 1.9
Outputs:
- result: bfloat16 [65536, 2048], P(('rep', 'fs'), 'tp')
All inputs are finite; a program needn't handle non-finite values.
Results may differ from a plain program's by a relative error of at most 0.013.
Values may be sent and summed in bfloat16 or wider, within the bound.
No kernel may reach another device: no remote copies, remote signals or barrier semaphores. Data moves between devices by JAX's collectives and lax.ppermute only.
A program may use at most 128 MiB of HBM per device.

v0:
```python
import jax
import jax.numpy as jnp
from jax import lax
from jax.sharding import PartitionSpec as P


def turned_gather(arrays, axis, dims):
    turned = [jnp.moveaxis(a, dim, 0) for a, dim in zip(arrays, dims)]
    widths = [t[0].size for t in turned]
    both = jnp.concatenate([t.reshape(-1, w) for t, w in zip(turned, widths)], axis=1)
    result = lax.all_gather(both, axis, axis=0, tiled=True)
    pieces = jnp.split(result, [sum(widths[:k]) for k in range(1, len(widths))], axis=1)
    return tuple(
        (
            jnp.moveaxis(b.reshape(-1, *t.shape[1:]), 0, dim)
            for b, t, dim in zip(pieces, turned, dims)
        )
    )


def in_one_piece(arrays, axis, dim, along):
    ends, at = ([], 0)
    for a in arrays[:-1]:
        at += a.shape[along]
        ends.append(at)
    both = jnp.concatenate(arrays, axis=along)
    return tuple(jnp.split(lax.all_gather(both, axis, axis=dim, tiled=True), ends, axis=along))


def copy_for_each(array, axis):
    copies = jnp.broadcast_to(array, (lax.axis_size(axis), *array.shape))
    return lax.all_to_all(copies, axis, split_axis=0, concat_axis=0, tiled=True)


def over_copies(array, axis):
    return copy_for_each(array, axis).sum(axis=0)


def packed_total(arrays, axis):
    vector, at, gathered = (jnp.concatenate([a.reshape(-1) for a in arrays]), 0, [])
    running = over_copies(vector, axis)
    for a in arrays:
        gathered.append(running[at : at + a.size].reshape(a.shape))
        at += a.size
    return tuple(gathered)


def in_order(pieces, dim):
    dims = list(pieces.shape[1:])
    dims[dim] *= pieces.shape[0]
    return jnp.moveaxis(pieces, 0, dim).reshape(dims)


def gathered_copies(array, axis, dim):
    pieces = copy_for_each(array, axis)
    return in_order(pieces, dim)


def total_of_pieces(array, axis):
    pieces = lax.all_gather(array, axis).astype(jnp.float32)
    return pieces.sum(axis=0)


def in_blocks(array, dim, peers):
    before, after = (array.shape[:dim], array.shape[dim + 1 :])
    return jnp.moveaxis(array.reshape(*before, peers, -1, *after), dim, 0)


def sent_and_summed(array, axis, dim):
    peers = lax.axis_size(axis)
    pieces = lax.all_to_all(in_blocks(array, dim, peers), axis, 0, 0, tiled=True)
    return jnp.sum(pieces.astype(jnp.float32), axis=0)


def rms_norm(values, gain, width, power_sum):
    return values * lax.rsqrt(power_sum / width + 1e-06) * gain


def local(
    resid,
    gain_mix_in,
    u_weight,
    v_weight,
    u_scale,
    v_scale,
    v_gain,
    mix_matrix,
    mix_bias,
    out_weight,
    out_scale,
    gain_mix_out,
    gain_ffn_in,
    up_weight,
    up_scale,
    down_weight,
    down_scale,
    gain_ffn_out,
):
    rows = resid.shape[0]
    part_width = resid.shape[1]
    width = part_width * lax.axis_size("tp")
    lane = lax.axis_index("tp")
    full_rows = lax.all_gather(resid, "tp", axis=1, tiled=True)
    out_scales, down_scales = turned_gather((out_scale, down_scale), "fs", (0, 0))
    full_float = full_rows.astype(jnp.float32)
    normed = rms_norm(
        full_float, gain_mix_in, width, jnp.sum(full_float * full_float, axis=1, keepdims=True)
    ).astype(jnp.bfloat16)
    branch_cols = u_weight.shape[1]
    pieces = in_one_piece(
        (u_weight.astype(jnp.bfloat16), v_weight.astype(jnp.bfloat16)), "fs", 0, 1
    )
    u_pre = jnp.dot(normed, pieces[0], preferred_element_type=jnp.float32)
    v_pre = jnp.dot(normed, pieces[1], preferred_element_type=jnp.float32)
    u_act = jax.nn.gelu(u_pre * u_scale)
    v_act = jax.nn.gelu(v_pre * v_scale)
    total, squares = packed_total(
        (jnp.sum(v_act, axis=1, keepdims=True), jnp.sum(v_act * v_act, axis=1, keepdims=True)), "tp"
    )
    branch_width = branch_cols * lax.axis_size("tp")
    centre = total / branch_width
    spread = squares / branch_width - centre * centre
    v_norm = ((v_act - centre) * lax.rsqrt(spread + 1e-06) * v_gain).astype(jnp.bfloat16)
    groups = mix_matrix.shape[0]
    block = mix_matrix.shape[1]
    blocks = v_norm.reshape(rows // block, block, groups, branch_cols // groups)
    mixed = (
        jnp.einsum(
            "gts,bsgd->btgd",
            mix_matrix.astype(jnp.bfloat16),
            blocks,
            preferred_element_type=jnp.float32,
        )
        + mix_bias.T[None, :, :, None]
    )
    gated = (u_act * mixed.reshape(rows, branch_cols)).astype(jnp.bfloat16)
    partial_value = jnp.dot(
        gated,
        gathered_copies(out_weight.astype(jnp.bfloat16), "fs", 1),
        preferred_element_type=jnp.float32,
    )
    mix_out = (
        total_of_pieces(partial_value.astype(jnp.bfloat16), "tp").astype(jnp.float32) * out_scales
    )
    power = jnp.sum(mix_out * mix_out, axis=1, keepdims=True)
    middle_full = (full_float + rms_norm(mix_out, gain_mix_out, width, power)).astype(jnp.bfloat16)
    middle = lax.dynamic_slice_in_dim(middle_full, lane * part_width, part_width, 1)
    middle_float = middle_full.astype(jnp.float32)
    ffn_in = rms_norm(
        middle_float,
        gain_ffn_in,
        width,
        jnp.sum(middle_float * middle_float, axis=1, keepdims=True),
    ).astype(jnp.bfloat16)
    up_half = up_weight.astype(jnp.bfloat16)
    down_half = down_weight.astype(jnp.bfloat16)
    whole_up = lax.all_gather(up_half, "fs", axis=0, tiled=True)
    raised = jnp.dot(ffn_in, whole_up, preferred_element_type=jnp.float32)
    hidden = jnp.square(jax.nn.relu(raised * up_scale)).astype(jnp.bfloat16)
    whole_down = lax.all_gather(down_half, "fs", axis=1, tiled=True)
    terms = jnp.dot(hidden, whole_down, preferred_element_type=jnp.float32)
    own_down = lax.dynamic_slice_in_dim(down_scales, lane * part_width, part_width, 0)
    ffn_out = sent_and_summed(terms.astype(jnp.bfloat16), "tp", 1) * own_down
    power_out = over_copies(jnp.sum(ffn_out * ffn_out, axis=1, keepdims=True), "tp")
    own_gain_out = lax.dynamic_slice_in_dim(gain_ffn_out, lane * part_width, part_width, 0)
    return (middle.astype(jnp.float32) + rms_norm(ffn_out, own_gain_out, width, power_out)).astype(
        jnp.bfloat16
    )


def solution(mesh):
    in_specs = (
        P(("rep", "fs"), "tp"),
        P(),
        P("fs", "tp"),
        P("fs", "tp"),
        P("tp"),
        P("tp"),
        P("tp"),
        P("tp", None, None),
        P("tp", None),
        P("tp", "fs"),
        P("fs"),
        P(),
        P(),
        P("fs", "tp"),
        P("tp"),
        P("tp", "fs"),
        P("fs"),
        P(),
    )
    out_specs = P(("rep", "fs"), "tp")
    return jax.shard_map(local, mesh=mesh, in_specs=in_specs, out_specs=out_specs, check_vma=False)
```

profile of v0, /device:TPU:1, one launch (start us, length us, event | category | flops | bytes accessed | tf_op | source)
XLA Modules:
  0.0 657.6 jit_solution(17726470480720936505)
XLA Ops:
  6.5 0.7 all-gather.8.cloned.1.call-update
  7.3 0.0 all-gather.10.cloned.1.call-start
  7.3 0.9 convert_element_type.62
  8.2 0.9 convert_element_type.63
  9.1 0.7 pad_maximum_fusion
  9.8 0.0 all-gather.10.cloned.1.call-update
  9.8 0.9 convert_element_type.67
  10.8 18.3 %all-gather.8.cloned.1.call-done = bf16[1024,2048]{1,0:T(8,128)(2,1)} async-done(((bf16[1024,1024]{1,0:T(8,128)(2,1)}), bf16[1024,2048]{1,0:T(8,128)(2,1)}) %all-gather.8.cloned.1.call-update) | async-done | bytes 4194320 | tf_op jit(solution)/shard_map/all_gather | solution.py:103
  29.0 3.1 fusion.3
  32.1 135.9 %all-gather.10.cloned.1.call-done = bf16[2048,1024]{1,0:T(8,128)(2,1)} async-done(((bf16[64,1024]{1,0:T(8,128)(2,1)}), bf16[2048,1024]{1,0:T(8,128)(2,1)}) %all-gather.10.cloned.1.call-update) | async-done | bytes 4194320 | tf_op jit(solution)/shard_map/all_gather | solution.py:27
  168.0 5.8 fusion.68
  173.8 24.0 %all_to_all.21 = f32[2,1,2048]{2,1,0:T(1,128)S(1)} all-to-all(f32[2,1,2048]{2,1,0:T(1,128)S(1)} %broadcast_in_dim.6), channel_id=1, replica_groups=mesh['rep'=2,'fs'=32,'tp'=2] {'tp'}, dimensions={0} | all-to-all | bytes 32768 | tf_op jit(solution)/shard_map/all_to_all | solution.py:32
  197.8 1.6 broadcast_in_dim.7
  199.4 7.1 %all-to-all-start.1 = ((bf16[32,512,64]{1,2,0:T(8,128)(2,1)}), bf16[32,512,64]{1,2,0:T(8,128)(2,1)}, u32[]{:S(2)}, u32[]{:S(2)}) async-start(bf16[32,512,64]{1,2,0:T(8,128)(2,1)} %broadcast_in_dim.7), calls=%async_computation.1 | async-start | bytes 4194304 | tf_op jit(solution)/shard_map/all_to_all | solution.py:32
  206.5 0.0 all-gather.16.cloned.1.call-start
  206.6 0.3 multiply_convert_fusion.1
  206.9 2.1 reshape.90
  209.1 2.4 bitcast_add_fusion
  211.5 2.7 copy.55
  214.2 3.4 reshape.91
  217.6 15.7 %all-to-all-done.1 = bf16[32,512,64]{1,2,0:T(8,128)(2,1)} async-done(((bf16[32,512,64]{1,2,0:T(8,128)(2,1)}), bf16[32,512,64]{1,2,0:T(8,128)(2,1)}, u32[]{:S(2)}, u32[]{:S(2)}) %all-to-all-start.1) | async-done | bytes 2097184 | tf_op jit(solution)/shard_map/all_to_all | solution.py:32
  233.4 10.3 %convolution_convert_fusion = bf16[1024,2048]{1,0:T(8,128)(2,1)} fusion(bf16[512,2048]{0,1:T(8,128)(2,1)} %bitcast.5, f32[1024,512]{1,0:T(8,128)S(1)} %reshape.91, bf16[2048,1024]{1,0:T(8,128)(2,1)} %all-gather.10.cloned.1.call-done, bf16[1024,2048]{1,0:T(8,128)(2,1)} %all-gather.8.cloned.1.call-done, f32[2048]{0:T(1024)S(1)} %copy-done.10, ...), kind=kOutput, calls=%fused_computation.24 | convolution fusion | flops 4311220224 | bytes 14694400 | tf_op jit(solution)/shard_map/dot_general | solution.py:137
  243.7 0.0 all-gather.16.cloned.1.call-update
  243.8 0.0 all-gather.12.cloned.1.call-start
  243.8 1.0 copy-done.3
  244.8 0.7 convert_element_type.74
  245.5 0.0 all-gather.12.cloned.1.call-update
  245.5 0.0 all-gather.14.cloned.1.call-start
  245.6 0.7 convert_element_type.76
  246.3 0.0 all-gather.14.cloned.1.call-update
  246.4 66.4 %all-gather.1 = f32[32,64,2]{1,2,0:T(2,128)S(1)} all-gather(f32[1,64,2]{1,2,0:T(2,128)S(1)} %maximum_bitcast_fusion), channel_id=1, replica_groups=mesh['rep'=2,'fs'=32,'tp'=2] {'fs'}, dimensions={0}, use_global_device_ids=true | all-gather | bytes 16896 | tf_op jit(solution)/shard_map/all_gather | solution.py:11
  312.8 0.1 reshape.88
  312.9 0.0 all-gather.16.cloned.1.call-done
  313.0 9.9 %convert_reduce_fusion = f32[1024,2048]{1,0:T(8,128)} fusion(bf16[2,1024,2048]{2,1,0:T(8,128)(2,1)} %bitcast.34), kind=kLoop, calls=%fused_computation | loop fusion | flops 6291456 | bytes 16777216 | tf_op jit(solution)/shard_map/reduce_sum | solution.py:61
  322.9 4.5 multiply_reduce_fusion
  327.5 1.3 copy-done
  328.8 4.0 fusion
  332.8 82.2 %all-gather.12.cloned.1.call-done = bf16[2048,2048]{1,0:T(8,128)(2,1)} async-done(((bf16[64,2048]{1,0:T(8,128)(2,1)}), bf16[2048,2048]{1,0:T(8,128)(2,1)}) %all-gather.12.cloned.1.call-update) | async-done | bytes 8388624 | tf_op jit(solution)/shard_map/all_gather | solution.py:157
  415.0 167.9 %all-gather.14.cloned.1.call-done = bf16[2048,2048]{0,1:T(8,128)(2,1)} async-done(((bf16[2048,64]{0,1:T(8,128)(2,1)}), bf16[2048,2048]{0,1:T(8,128)(2,1)}) %all-gather.14.cloned.1.call-update) | async-done | bytes 8388624 | tf_op jit(solution)/shard_map/all_gather | solution.py:160
  582.9 25.7 %fusion.16 = bf16[1024,2048]{1,0:T(8,128)(2,1)} fusion(bf16[2048,2048]{0,1:T(8,128)(2,1)} %all-gather.14.cloned.1.call-done, bf16[2048,2048]{1,0:T(8,128)(2,1)} %all-gather.12.cloned.1.call-done, bf16[1024,2048]{1,0:T(8,128)(2,1)} %get-tuple-element.8, f32[2048]{0:T(1024)S(1)} %copy-done.11, f32[2048]{0:T(1024)S(1)} %copy-done.12, f32[1024]{0:T(1024)S(1)} %add_rsqrt_fusion.1), kind=kOutput, calls=%fused_computation.25 | convolution fusion | flops 17198743552 | bytes 25186304 | tf_op jit(solution)/shard_map/dot_general | solution.py:161
  608.5 2.6 copy.66
  611.2 27.7 %all_to_all.22 = bf16[2,1024,1024]{2,1,0:T(8,128)(2,1)S(1)} all-to-all(bf16[2,1024,1024]{2,1,0:T(8,128)(2,1)S(1)} %bitcast.33), channel_id=1, replica_groups=mesh['rep'=2,'fs'=32,'tp'=2] {'tp'}, dimensions={0} | all-to-all | bytes 8388608 | tf_op jit(solution)/shard_map/all_to_all | solution.py:71
  638.8 1.0 convert_reduce_fusion.1
  639.9 0.0 dynamic-slice-start
  639.9 1.9 copy-done.1
  641.8 0.5 multiply_reduce_fusion.1
  642.3 3.7 all_to_all.23
  646.1 5.0 add_convert_fusion
  (43 shorter events, 0.2 us)
Async XLA Ops:
  6.5 161.5 %copy-start.10 = (f32[2048]{0:T(1024)S(1)}, f32[2048]{0:T(1024)}, u32[]{:S(2)}) copy-start(f32[2048]{0:T(1024)} %param.19) | copy-start | bytes 24580
  6.5 161.5 %copy-start.13 = (f32[512]{0:T(512)S(1)}, f32[512]{0:T(512)}, u32[]{:S(2)}) copy-start(f32[512]{0:T(512)} %param.23) | copy-start | bytes 6148
  6.5 22.5 %all-gather.8.cloned.1.call-start = ((), (), s32[]{:S(2)}) async-start(), calls=%async_computation.4 | async-start | bytes 6291456 | tf_op jit(solution)/shard_map/all_gather | solution.py:103
  7.3 160.7 %all-gather.10.cloned.1.call-start = ((), (), s32[]{:S(2)}) async-start(), calls=%async_computation.5 | async-start | bytes 4325376 | tf_op jit(solution)/shard_map/all_gather | solution.py:27
  173.8 32.8 %copy-start.7 = (f32[512]{0:T(512)S(1)}, f32[512]{0:T(512)}, u32[]{:S(2)}) copy-start(f32[512]{0:T(512)} %param.24) | copy-start | bytes 6148
  199.4 34.0 %all-to-all-start.1 = ((bf16[32,512,64]{1,2,0:T(8,128)(2,1)}), bf16[32,512,64]{1,2,0:T(8,128)(2,1)}, u32[]{:S(2)}, u32[]{:S(2)}) async-start(bf16[32,512,64]{1,2,0:T(8,128)(2,1)} %broadcast_in_dim.7), calls=%async_computation.1 | async-start | bytes 4194304 | tf_op jit(solution)/shard_map/all_to_all | solution.py:32
  206.5 2.6 copy-start.6
  206.5 106.5 %all-gather.16.cloned.1.call-start = ((), (), s32[]{:S(2)}) async-start(), calls=%async_computation.8 | async-start | bytes 12582912 | tf_op jit(solution)/shard_map/all_gather | solution.py:60
  214.2 19.2 %copy-start.14 = (f32[512]{0:T(512)S(1)}, f32[512]{0:T(512)}, u32[]{:S(2)}) copy-start(f32[512]{0:T(512)} %param.22) | copy-start | bytes 6148
  243.7 1.0 copy-start.3
  243.7 1.9 copy-start.4
  243.7 2.6 copy-start.8
  243.7 2.6 copy-start.9
  243.8 171.2 %all-gather.12.cloned.1.call-start = ((), (), s32[]{:S(2)}) async-start(), calls=%async_computation.6 | async-start | bytes 8650752 | tf_op jit(solution)/shard_map/all_gather | solution.py:157
  245.5 337.3 %all-gather.14.cloned.1.call-start = ((), (), s32[]{:S(2)}) async-start(), calls=%async_computation.7 | async-start | bytes 8650752 | tf_op jit(solution)/shard_map/all_gather | solution.py:160
  313.0 14.5 %copy-start.2 = (bf16[1024,2048]{1,0:T(8,128)(2,1)S(1)}, bf16[1024,2048]{1,0:T(8,128)(2,1)}, u32[]{:S(2)}) copy-start(bf16[1024,2048]{1,0:T(8,128)(2,1)} %all-gather.8.cloned.1.call-done) | copy-start | bytes 12582916
  322.9 5.9 copy-start
  322.9 5.9 copy-start.5
  328.8 254.1 %copy-start.11 = (f32[2048]{0:T(1024)S(1)}, f32[2048]{0:T(1024)}, u32[]{:S(2)}) copy-start(f32[2048]{0:T(1024)} %param.32) | copy-start | bytes 24580
  328.8 254.1 %copy-start.12 = (f32[2048]{0:T(1024)S(1)}, f32[2048]{0:T(1024)}, u32[]{:S(2)}) copy-start(f32[2048]{0:T(1024)} %param.30) | copy-start | bytes 24580
  639.9 1.9 copy-start.1
  639.9 6.2 dynamic-slice-start
Sparse Core Ops, SparseCore 0:
  9.0 19.9 all-gather.7
  30.7 137.2 all-gather.9
  243.9 22.8 all-gather.15
  268.3 146.6 all-gather.11
  416.4 166.3 all-gather.13
where the time goes:
time: 658 us
  waiting for transfers between devices  421 us (64%)
  blocking collectives  122 us (19%)
  matrix products  44.2 us (7%)
  other arithmetic  33.3 us (5%)
  local copies, waits for them, and re-layouts  16.9 us (3%)
  between operations  13.4 us (2%)
  starting transfers between devices  7.24 us (1%)
    all_gather x1, waiting for transfers between devices, local(): whole_down = lax.all_gather(down_half, 'fs', axis=1, tiled=True)  168 us
    all_gather x1, waiting for transfers between devices, in_one_piece(): lax.all_gather(both, axis, axis=dim, tiled=True)  136 us
    all_gather x1, waiting for transfers between devices, local(): whole_up = lax.all_gather(up_half, 'fs', axis=0, tiled=True)  82.2 us
    all_gather x1, blocking collectives, turned_gather(): result = lax.all_gather(both, axis, axis=0, tiled=True)  66.4 us
    all_to_all x2, blocking collectives, copy_for_each(): return lax.all_to_all(copies, axis, split_axis=0, concat_axis=0, tiled=True)  27.7 us
    all_to_all x1, blocking collectives, sent_and_summed(): lax.all_to_all(in_blocks(array, dim, peers), axis, 0, 0, tiled=True)  27.7 us
    dot_general x1, matrix products, local(): terms = jnp.dot(hidden, whole_down, preferred_element_type=jnp.float32)  25.7 us
    all_gather x1, waiting for transfers between devices, local(): full_rows = lax.all_gather(resid, 'tp', axis=1, tiled=True)  18.3 us
  transfers between devices with their start and end apart: 6, of which 5 were waited for; matrix products, arithmetic and copies ran while one was open for 6% of the time, Pallas kernels for 0%

commit v1 on v0

--- a/solution.py
+++ b/solution.py
@@ -157,7 +157,7 @@
     whole_up = lax.all_gather(up_half, "fs", axis=0, tiled=True)
     raised = jnp.dot(ffn_in, whole_up, preferred_element_type=jnp.float32)
     hidden = jnp.square(jax.nn.relu(raised * up_scale)).astype(jnp.bfloat16)
-    whole_down = lax.all_gather(down_half, "fs", axis=1, tiled=True)
+    whole_down = jnp.concatenate(lax.all_gather(down_half, "fs"), axis=1)
     terms = jnp.dot(hidden, whole_down, preferred_element_type=jnp.float32)
     own_down = lax.dynamic_slice_in_dim(down_scales, lane * part_width, part_width, 0)
     ffn_out = sent_and_summed(terms.astype(jnp.bfloat16), "tp", 1) * own_down

time: 658 us -> 628 us (0.954); the launches traced: 658 us -> 619 us
  waiting for transfers between devices: 421 us -> 354 us
  local copies, waits for them, and re-layouts: 16.9 us -> 40.2 us
    all_gather x1, waiting for transfers between devices: 168 us -> 24.6 us  [local(): whole_down = jnp.concatenate(lax.all_gather(down_half, 'fs'), axis=1)]
    all_gather x1, waiting for transfers between devices: 82.2 us -> 128 us  [local(): whole_up = lax.all_gather(up_half, 'fs', axis=0, tiled=True)]
    all_gather x1, waiting for transfers between devices: 0.02 us -> 19 us  [total_of_pieces(): pieces = lax.all_gather(array, axis).astype(jnp.float32)]
    all_to_all x1, waiting for transfers between devices: 15.7 us -> 28.9 us  [copy_for_each(): return lax.all_to_all(copies, axis, split_axis=0, concat_axis=0, tiled=True)]
    unnamed x31 -> x30, local copies, waits for them, and re-layouts: 4.35 us -> 16.4 us
    reshape x0 -> x1, local copies, waits for them, and re-layouts: none -> 11.2 us  [local(): whole_down = jnp.concatenate(lax.all_gather(down_half, 'fs'), axis=1)]
  transfers between devices with their start and end apart: 6 -> 6, of which waited for: 5 -> 6; matrix products, arithmetic and copies ran while one was open for 6% -> 13% of each run, Pallas kernels for 0% -> 0%
where the time goes in v1:
time: 628 us; the launch traced here: 619 us
  waiting for transfers between devices  354 us (56%)
  blocking collectives  126 us (20%)
  matrix products  44.2 us (7%)
  local copies, waits for them, and re-layouts  40.2 us (6%)
  other arithmetic  34.5 us (5%)
  between operations  13.6 us (2%)
  starting transfers between devices  7.24 us (1%)
    all_gather x1, waiting for transfers between devices, in_one_piece(): lax.all_gather(both, axis, axis=dim, tiled=True)  136 us
    all_gather x1, waiting for transfers between devices, local(): whole_up = lax.all_gather(up_half, 'fs', axis=0, tiled=True)  128 us
    all_gather x1, blocking collectives, turned_gather(): result = lax.all_gather(both, axis, axis=0, tiled=True)  70 us
    all_to_all x1, waiting for transfers between devices, copy_for_each(): return lax.all_to_all(copies, axis, split_axis=0, concat_axis=0, tiled=True)  28.9 us
    all_to_all x1, blocking collectives, sent_and_summed(): lax.all_to_all(in_blocks(array, dim, peers), axis, 0, 0, tiled=True)  27.9 us
    all_to_all x2, blocking collectives, copy_for_each(): return lax.all_to_all(copies, axis, split_axis=0, concat_axis=0, tiled=True)  27.7 us
    dot_general x1, matrix products, local(): terms = jnp.dot(hidden, whole_down, preferred_element_type=jnp.float32)  25.7 us
    all_gather x1, waiting for transfers between devices, local(): whole_down = jnp.concatenate(lax.all_gather(down_half, 'fs'), axis=1)  24.6 us
  transfers between devices with their start and end apart: 6, of which 6 were waited for; matrix products, arithmetic and copies ran while one was open for 13% of the time, Pallas kernels for 0%

profile of v1, /device:TPU:1, one launch (start us, length us, event | category | flops | bytes accessed | tf_op | source)
XLA Modules:
  0.0 619.3 jit_solution(17536414373263872581)
XLA Ops:
  6.5 0.7 all-gather.9.cloned.1.call-update
  7.3 0.0 all-gather.11.cloned.1.call-start
  7.3 0.9 convert_element_type.62
  8.2 0.9 convert_element_type.63
  9.1 0.7 pad_maximum_fusion
  9.8 0.0 all-gather.11.cloned.1.call-update
  9.8 0.0 all-gather.17.cloned.1.call-start
  9.9 1.8 convert_element_type.76
  11.7 0.0 all-gather.17.cloned.1.call-update
  11.7 0.9 convert_element_type.67
  12.6 16.4 %all-gather.9.cloned.1.call-done = bf16[1024,2048]{1,0:T(8,128)(2,1)} async-done(((bf16[1024,1024]{1,0:T(8,128)(2,1)}), bf16[1024,2048]{1,0:T(8,128)(2,1)}) %all-gather.9.cloned.1.call-update) | async-done | bytes 4194320 | tf_op jit(solution)/shard_map/all_gather | solution.py:103
  29.0 3.1 fusion.3
  32.1 135.9 %all-gather.11.cloned.1.call-done = bf16[2048,1024]{1,0:T(8,128)(2,1)} async-done(((bf16[64,1024]{1,0:T(8,128)(2,1)}), bf16[2048,1024]{1,0:T(8,128)(2,1)}) %all-gather.11.cloned.1.call-update) | async-done | bytes 4194320 | tf_op jit(solution)/shard_map/all_gather | solution.py:27
  168.0 5.8 fusion.68
  173.8 24.0 %all_to_all.21 = f32[2,1,2048]{2,1,0:T(1,128)S(1)} all-to-all(f32[2,1,2048]{2,1,0:T(1,128)S(1)} %broadcast_in_dim.6), channel_id=1, replica_groups=mesh['rep'=2,'fs'=32,'tp'=2] {'tp'}, dimensions={0} | all-to-all | bytes 32768 | tf_op jit(solution)/shard_map/all_to_all | solution.py:32
  197.8 1.6 broadcast_in_dim.7
  199.4 7.1 %all-to-all-start.1 = ((bf16[32,512,64]{1,2,0:T(8,128)(2,1)}), bf16[32,512,64]{1,2,0:T(8,128)(2,1)}, u32[]{:S(2)}, u32[]{:S(2)}) async-start(bf16[32,512,64]{1,2,0:T(8,128)(2,1)} %broadcast_in_dim.7), calls=%async_computation.1 | async-start | bytes 4194304 | tf_op jit(solution)/shard_map/all_to_all | solution.py:32
  206.5 0.0 all-gather.15.cloned.1.call-start
  206.6 0.3 multiply_convert_fusion.1
  206.9 2.1 reshape.99
  209.1 2.4 bitcast_add_fusion
  211.5 2.8 copy.65
  214.2 3.4 reshape.100
  217.7 28.9 %all-to-all-done.1 = bf16[32,512,64]{1,2,0:T(8,128)(2,1)} async-done(((bf16[32,512,64]{1,2,0:T(8,128)(2,1)}), bf16[32,512,64]{1,2,0:T(8,128)(2,1)}, u32[]{:S(2)}, u32[]{:S(2)}) %all-to-all-start.1) | async-done | bytes 2097184 | tf_op jit(solution)/shard_map/all_to_all | solution.py:32
  246.5 10.4 %convolution_convert_fusion = bf16[1024,2048]{1,0:T(8,128)(2,1)} fusion(bf16[512,2048]{0,1:T(8,128)(2,1)} %bitcast.5, f32[1024,512]{1,0:T(8,128)S(1)} %reshape.100, bf16[2048,1024]{1,0:T(8,128)(2,1)} %all-gather.11.cloned.1.call-done, bf16[1024,2048]{1,0:T(8,128)(2,1)} %all-gather.9.cloned.1.call-done, f32[2048]{0:T(1024)S(1)} %copy-done.9, ...), kind=kOutput, calls=%fused_computation.24 | convolution fusion | flops 4311220224 | bytes 14694400 | tf_op jit(solution)/shard_map/dot_general | solution.py:137
  256.9 0.0 all-gather.15.cloned.1.call-update
  256.9 0.0 all-gather.13.cloned.1.call-start
  257.0 1.0 copy-done.3
  257.9 0.7 convert_element_type.74
  258.7 70.0 %all-gather.2 = f32[32,64,2]{1,2,0:T(2,128)S(1)} all-gather(f32[1,64,2]{1,2,0:T(2,128)S(1)} %maximum_bitcast_fusion), channel_id=1, replica_groups=mesh['rep'=2,'fs'=32,'tp'=2] {'fs'}, dimensions={0}, use_global_device_ids=true | all-gather | bytes 16896 | tf_op jit(solution)/shard_map/all_gather | solution.py:11
  328.8 0.1 reshape.97
  328.9 24.6 %all-gather.17.cloned.1.call-done = bf16[65536,64]{0,1:T(8,128)(2,1)} async-done(((bf16[2048,64]{0,1:T(8,128)(2,1)}), bf16[65536,64]{0,1:T(8,128)(2,1)}) %all-gather.17.cloned.1.call-update) | async-done | bytes 8388624 | tf_op jit(solution)/shard_map/all_gather | solution.py:160
  353.5 12.1 %copy.71 = bf16[8,8,32,2048]{3,2,1,0:T(8,128)(2,1)} copy(bf16[8,8,32,2048]{3,1,2,0:T(8,128)(2,1)} %bitcast.42) | data formatting | bytes 16777216
  365.6 11.2 %copy.59 = bf16[2048,32,64]{0,2,1:T(8,128)(2,1)} copy(bf16[2048,32,64]{0,1,2:T(8,128)(2,1)} %bitcast.40) | data formatting | bytes 16777216 | tf_op jit(solution)/shard_map/reshape | solution.py:160
  376.8 19.0 %all-gather.15.cloned.1.call-done = bf16[2048,2048]{1,0:T(8,128)(2,1)} async-done(((bf16[1024,2048]{1,0:T(8,128)(2,1)}), bf16[2048,2048]{1,0:T(8,128)(2,1)}) %all-gather.15.cloned.1.call-update) | async-done | bytes 8388624 | tf_op jit(solution)/shard_map/all_gather | solution.py:60
  395.8 10.0 %convert_reduce_fusion = f32[1024,2048]{1,0:T(8,128)} fusion(bf16[2,1024,2048]{2,1,0:T(8,128)(2,1)} %bitcast.43), kind=kLoop, calls=%fused_computation | loop fusion | flops 6291456 | bytes 16777216 | tf_op jit(solution)/shard_map/reduce_sum | solution.py:61
  405.8 4.5 multiply_reduce_fusion
  410.4 1.3 copy-done
  411.7 4.0 fusion
  415.7 128.4 %all-gather.13.cloned.1.call-done = bf16[2048,2048]{1,0:T(8,128)(2,1)} async-done(((bf16[64,2048]{1,0:T(8,128)(2,1)}), bf16[2048,2048]{1,0:T(8,128)(2,1)}) %all-gather.13.cloned.1.call-update) | async-done | bytes 8388624 | tf_op jit(solution)/shard_map/all_gather | solution.py:157
  544.1 25.7 %fusion.16 = bf16[1024,2048]{1,0:T(8,128)(2,1)} fusion(bf16[2048,2048]{0,1:T(8,128)(2,1)} %bitcast.44, bf16[2048,2048]{1,0:T(8,128)(2,1)} %all-gather.13.cloned.1.call-done, bf16[1024,2048]{1,0:T(8,128)(2,1)} %get-tuple-element.8, f32[2048]{0:T(1024)S(1)} %copy-done.10, f32[2048]{0:T(1024)S(1)} %copy-done.11, f32[1024]{0:T(1024)S(1)} %add_rsqrt_fusion.1), kind=kOutput, calls=%fused_computation.25 | convolution fusion | flops 17198743552 | bytes 25186304 | tf_op jit(solution)/shard_map/dot_general | solution.py:161
  569.8 2.6 copy.77
  572.4 27.9 %all_to_all.22 = bf16[2,1024,1024]{2,1,0:T(8,128)(2,1)S(1)} all-to-all(bf16[2,1024,1024]{2,1,0:T(8,128)(2,1)S(1)} %bitcast.41), channel_id=1, replica_groups=mesh['rep'=2,'fs'=32,'tp'=2] {'tp'}, dimensions={0} | all-to-all | bytes 8388608 | tf_op jit(solution)/shard_map/all_to_all | solution.py:71
  600.3 1.0 convert_reduce_fusion.1
  601.4 1.9 copy-done.1
  603.3 0.5 multiply_reduce_fusion.1
  603.8 3.7 all_to_all.23
  607.6 5.0 add_convert_fusion
  (43 shorter events, 0.2 us)
Async XLA Ops:
  6.5 161.5 %copy-start.9 = (f32[2048]{0:T(1024)S(1)}, f32[2048]{0:T(1024)}, u32[]{:S(2)}) copy-start(f32[2048]{0:T(1024)} %param.19) | copy-start | bytes 24580
  6.5 161.5 %copy-start.12 = (f32[512]{0:T(512)S(1)}, f32[512]{0:T(512)}, u32[]{:S(2)}) copy-start(f32[512]{0:T(512)} %param.23) | copy-start | bytes 6148
  6.5 22.5 %all-gather.9.cloned.1.call-start = ((), (), s32[]{:S(2)}) async-start(), calls=%async_computation.4 | async-start | bytes 6291456 | tf_op jit(solution)/shard_map/all_gather | solution.py:103
  7.3 160.7 %all-gather.11.cloned.1.call-start = ((), (), s32[]{:S(2)}) async-start(), calls=%async_computation.5 | async-start | bytes 4325376 | tf_op jit(solution)/shard_map/all_gather | solution.py:27
  9.8 343.7 %all-gather.17.cloned.1.call-start = ((), (), s32[]{:S(2)}) async-start(), calls=%async_computation.8 | async-start | bytes 8650752 | tf_op jit(solution)/shard_map/all_gather | solution.py:160
  173.8 32.8 %copy-start.6 = (f32[512]{0:T(512)S(1)}, f32[512]{0:T(512)}, u32[]{:S(2)}) copy-start(f32[512]{0:T(512)} %param.24) | copy-start | bytes 6148
  199.4 47.1 %all-to-all-start.1 = ((bf16[32,512,64]{1,2,0:T(8,128)(2,1)}), bf16[32,512,64]{1,2,0:T(8,128)(2,1)}, u32[]{:S(2)}, u32[]{:S(2)}) async-start(bf16[32,512,64]{1,2,0:T(8,128)(2,1)} %broadcast_in_dim.7), calls=%async_computation.1 | async-start | bytes 4194304 | tf_op jit(solution)/shard_map/all_to_all | solution.py:32
  206.5 2.6 copy-start.5
  206.5 189.3 %all-gather.15.cloned.1.call-start = ((), (), s32[]{:S(2)}) async-start(), calls=%async_computation.7 | async-start | bytes 12582912 | tf_op jit(solution)/shard_map/all_gather | solution.py:60
  214.2 32.3 %copy-start.13 = (f32[512]{0:T(512)S(1)}, f32[512]{0:T(512)}, u32[]{:S(2)}) copy-start(f32[512]{0:T(512)} %param.22) | copy-start | bytes 6148
  256.9 1.0 copy-start.3
  256.9 1.8 copy-start.7
  256.9 1.8 copy-start.8
  256.9 287.2 %all-gather.13.cloned.1.call-start = ((), (), s32[]{:S(2)}) async-start(), calls=%async_computation.6 | async-start | bytes 8650752 | tf_op jit(solution)/shard_map/all_gather | solution.py:157
  395.8 14.6 %copy-start.2 = (bf16[1024,2048]{1,0:T(8,128)(2,1)S(1)}, bf16[1024,2048]{1,0:T(8,128)(2,1)}, u32[]{:S(2)}) copy-start(bf16[1024,2048]{1,0:T(8,128)(2,1)} %all-gather.9.cloned.1.call-done) | copy-start | bytes 12582916
  405.8 5.9 copy-start
  405.8 5.9 copy-start.4
  411.7 132.4 %copy-start.10 = (f32[2048]{0:T(1024)S(1)}, f32[2048]{0:T(1024)}, u32[]{:S(2)}) copy-start(f32[2048]{0:T(1024)} %param.32) | copy-start | bytes 24580
  411.7 132.4 %copy-start.11 = (f32[2048]{0:T(1024)S(1)}, f32[2048]{0:T(1024)}, u32[]{:S(2)}) copy-start(f32[2048]{0:T(1024)} %param.30) | copy-start | bytes 24580
  601.3 1.9 copy-start.1
  601.4 6.2 %dynamic-slice-start = ((f32[2048]{0:T(1024)}, s32[]{:T(128)}), f32[1024]{0:T(1024)S(1)}, s32[]{:S(2)}) async-start(f32[2048]{0:T(1024)} %param.35, s32[]{:T(128)} %select_n.2), calls=%async_computation.9 | async-start | bytes 8704 | tf_op jit(solution)/shard_map/dynamic_slice | solution.py:165
Sparse Core Ops, SparseCore 0:
  9.0 19.9 all-gather.8
  30.7 137.2 all-gather.10
  169.6 183.7 all-gather.16
  355.0 40.7 all-gather.14
  397.3 146.7 all-gather.12
